TPU v7x, 32 devices: a whole 2x2x4 slice. The times are simulated.
32 devices in a mesh: tp: 8 (over z, y), dp: 4 (over x, core).
Axes of the slice: x: 2, y: 2, z: 4, core: 2. Of those that a mesh axis runs over, the one named last changes fastest.
Arguments:
- stream: bfloat16 [128, 4096], P(None, ('dp', 'tp')), may hold values from -16 to 16
- lengths: int32 [128], P('dp'), may hold values from 1 to 64, 1024 in all
- prior_state: float32 [2, 128, 4096], P(None, 'dp', 'tp'), may hold values from -6 to 6
- prior_window: bfloat16 [2, 128, 3, 4096], P(None, 'dp', None, 'tp'), may hold values from -6 to 6
- norm_gain: float32 [2, 4096], P(None, 'dp'), may hold values from 0.1 to 1.9
- w_branch: bfloat16 [2, 4096, 4096], P(None, 'dp', 'tp'), may hold values from -0.09375 to 0.09375
- w_gate_branch: bfloat16 [2, 4096, 4096], P(None, 'dp', 'tp'), may hold values from -0.09375 to 0.09375
- conv_taps: bfloat16 [2, 4, 4096], P(None, None, 'tp'), may hold values from -3 to 3
- w_in_gate: bfloat16 [2, 256, 4096], P(None, None, 'tp'), may hold values from -0.375 to 0.375
- w_rec_gate: bfloat16 [2, 256, 4096], P(None, None, 'tp'), may hold values from -0.375 to 0.375
- decay_param: float32 [2, 4096], P(None, 'tp'), may hold values from -1 to 4
- w_out: bfloat16 [2, 4096, 4096], P(None, 'tp', 'dp'), may hold values from -0.1875 to 0.1875
Outputs:
- mixed_out: bfloat16 [128, 4096], P(None, ('dp', 'tp'))
- new_state: float32 [2, 128, 4096], P(None, 'dp', 'tp')
- new_window: bfloat16 [2, 128, 3, 4096], P(None, 'dp', None, 'tp')
All inputs are finite; a program needn't handle non-finite values. No bound on the sum of `lengths` on one device may be relied on, other than what follows from the above.
Results may differ from a plain program's by a relative error of at most 0.014.
Values may be sent and summed in bfloat16 or wider, within the bound.
A program may use at most 64 MiB of HBM per device.

v0:
```python
import jax
import jax.numpy as jnp
from jax import lax
from jax.sharding import PartitionSpec as P

D = 4096
BLOCK = 256
epsilon = 1e-06


def from_partner(block, axis, apart):
    count = lax.axis_size(axis)
    route = []
    for low in range(count):
        high = low | 1 << apart
        if high != low and high < count:
            route += [(low, high), (high, low)]
    return lax.ppermute(block, axis, route)


def norm_rows(block_rows, gain_values, squares):
    scaling = lax.rsqrt(squares / D + epsilon)
    return (block_rows.astype(jnp.float32) * scaling * gain_values).astype(jnp.bfloat16)


def normed_input(stream_local, gain_block):
    own_width = stream_local.shape[1]
    offset = lax.axis_index("tp") * own_width
    widened = stream_local.astype(jnp.float32)
    squares = lax.psum(jnp.sum(widened * widened, axis=1, keepdims=True), ("tp", "dp"))
    own_gain = lax.dynamic_slice_in_dim(gain_block, offset, own_width, 0)
    result = lax.all_gather(norm_rows(stream_local, own_gain, squares), "tp", axis=1, tiled=True)
    return result


def peer_block(convolved):
    col_count = convolved.shape[1]
    group_size = max(BLOCK // col_count, 1)
    device = lax.axis_index("tp")
    grouped = convolved
    for bit_number in range(group_size.bit_length() - 1):
        partner = from_partner(grouped, "tp", bit_number)
        is_upper = device // (1 << bit_number) % 2 == 1
        grouped = jnp.where(
            is_upper,
            jnp.concatenate([partner, grouped], axis=1),
            jnp.concatenate([grouped, partner], axis=1),
        )
    return grouped


def block_gates(grouped, weight):
    row_count = grouped.shape[0]
    col_count = weight.shape[1]
    blocks = max(col_count // BLOCK, 1)
    block_cols = min(col_count, BLOCK)
    inputs = grouped.reshape(row_count, blocks, BLOCK)
    tables = weight.reshape(BLOCK, blocks, block_cols)
    mapped = jnp.einsum("rnk,knc->rnc", inputs, tables, preferred_element_type=jnp.float32)
    return mapped.reshape(row_count, col_count)


def recurrent_step(
    normed,
    lengths,
    prior_state,
    prior_window,
    w_branch,
    w_gate_branch,
    conv_taps,
    w_in_gate,
    w_rec_gate,
    decay_param,
    w_out,
    stream_local,
):
    col_count = w_branch.shape[1]
    summed = lax.psum_scatter(
        jnp.concatenate(
            [
                jnp.dot(normed, w_branch, preferred_element_type=jnp.float32),
                jnp.dot(normed, w_gate_branch, preferred_element_type=jnp.float32),
            ],
            axis=1,
        ).astype(jnp.bfloat16),
        "dp",
        scatter_dimension=0,
        tiled=True,
    ).astype(jnp.float32)
    branch = summed[:, :col_count].astype(jnp.bfloat16)
    gate_in = summed[:, col_count:].astype(jnp.bfloat16)
    depth = prior_window.shape[1]
    needed = depth + 1 - jnp.arange(depth, dtype=jnp.int32)
    living = lengths[:, None, None] >= needed[None, :, None]
    history = jnp.where(living, prior_window, jnp.zeros_like(prior_window))
    window = jnp.concatenate([history, branch[:, None, :]], axis=1)
    convolved = jnp.sum(
        window.astype(jnp.float32) * conv_taps.astype(jnp.float32)[None], axis=1
    ).astype(jnp.bfloat16)
    grouped = peer_block(convolved)
    input_gate = jax.nn.sigmoid(block_gates(grouped, w_in_gate))
    recur_gate = jax.nn.sigmoid(block_gates(grouped, w_rec_gate))
    log_keep = 8.0 * recur_gate * jax.nn.log_sigmoid(decay_param)
    keeping = jnp.exp(log_keep)
    feeding = jnp.sqrt(-jnp.expm1(2.0 * log_keep))
    earlier = jnp.where(lengths[:, None] >= 2, prior_state, jnp.zeros_like(prior_state))
    state = keeping * earlier + feeding * input_gate * convolved.astype(jnp.float32)
    readout = (state * jax.nn.gelu(gate_in.astype(jnp.float32))).astype(jnp.bfloat16)
    mixed = jnp.dot(
        lax.all_gather(readout, "dp", axis=0, tiled=True), w_out, preferred_element_type=jnp.float32
    )
    own_width = stream_local.shape[1]
    offset = lax.axis_index("tp") * own_width
    own_cols = lax.dynamic_slice_in_dim(mixed, offset, own_width, 1) + stream_local.astype(
        jnp.float32
    )
    terms = lax.dynamic_update_slice_in_dim(mixed, own_cols, offset, 1)
    return (terms, state, window[:, 1:])


def body(
    stream,
    lengths,
    prior_state,
    prior_window,
    norm_gain,
    w_branch,
    w_gate_branch,
    conv_taps,
    w_in_gate,
    w_rec_gate,
    decay_param,
    w_out,
):
    normed = normed_input(stream, norm_gain[0])
    terms, state_first, window_first = recurrent_step(
        normed,
        lengths,
        prior_state[0],
        prior_window[0],
        w_branch[0],
        w_gate_branch[0],
        conv_taps[0],
        w_in_gate[0],
        w_rec_gate[0],
        decay_param[0],
        w_out[0],
        stream,
    )
    carried = lax.psum(terms, "tp").astype(jnp.bfloat16)
    widened = carried.astype(jnp.float32)
    squares = lax.psum(jnp.sum(widened * widened, axis=1, keepdims=True), "dp")
    normed = norm_rows(carried, norm_gain[1], squares)
    own_width = stream.shape[1]
    first = lax.dynamic_slice_in_dim(carried, lax.axis_index("tp") * own_width, own_width, 1)
    terms, state_second, window_second = recurrent_step(
        normed,
        lengths,
        prior_state[1],
        prior_window[1],
        w_branch[1],
        w_gate_branch[1],
        conv_taps[1],
        w_in_gate[1],
        w_rec_gate[1],
        decay_param[1],
        w_out[1],
        first,
    )
    second = lax.psum_scatter(terms, "tp", scatter_dimension=1, tiled=True).astype(jnp.bfloat16)
    return (
        second,
        jnp.stack([state_first, state_second]),
        jnp.stack([window_first, window_second]),
    )


def solution(mesh):
    placed = (
        P(None, ("dp", "tp")),
        P("dp"),
        P(None, "dp", "tp"),
        P(None, "dp", None, "tp"),
        P(None, "dp"),
        P(None, "dp", "tp"),
        P(None, "dp", "tp"),
        P(None, None, "tp"),
        P(None, None, "tp"),
        P(None, None, "tp"),
        P(None, "tp"),
        P(None, "tp", "dp"),
    )
    return jax.shard_map(
        body,
        mesh=mesh,
        in_specs=placed,
        out_specs=(P(None, ("dp", "tp")), P(None, "dp", "tp"), P(None, "dp", None, "tp")),
        check_vma=False,
    )
```

profile of v0, /device:TPU:0, one launch (start us, length us, event | category | flops | bytes accessed | tf_op | source)
XLA Modules:
  0.0 261.5 jit_solution(7721415944423887952)
XLA Ops:
  7.2 0.9 fusion.45
  8.1 42.0 %psum.21 = f32[128,1]{0,1:T(1,128)S(1)} all-reduce(f32[128,1]{0,1:T(1,128)S(1)} %bitcast.133), channel_id=1, replica_groups=mesh['tp'=8,'dp'=4] {'tp','dp'}, use_global_device_ids=true, to_apply=%region_1.0 | all-reduce | flops 128 | bytes 1024 | tf_op jit(solution)/shard_map/psum | solution.py:30
  50.1 1.4 fusion.76
  52.3 26.4 %all_gather.9 = bf16[128,1024]{1,0:T(8,128)(2,1)S(1)} all-gather(bf16[128,128]{1,0:T(8,128)(2,1)S(1)} %fusion.47), channel_id=1, replica_groups=mesh['tp'=8,'dp'=4] {'tp'}, dimensions={1}, use_global_device_ids=true | all-gather | bytes 294912 | tf_op jit(solution)/shard_map/all_gather | solution.py:32
  78.7 1.6 convolution_convert_fusion.2
  80.4 1.5 convolution_convert_fusion.3
  82.8 1.2 fusion.74
  85.7 1.0 bitcast_select_fusion.1
  86.8 14.5 %reduce-scatter.4.cloned.1.call-done = bf16[32,1024]{1,0:T(8,128)(2,1)} async-done(((bf16[128,1024]{1,0:T(8,128)(2,1)}), bf16[32,1024]{1,0:T(8,128)(2,1)}) %reduce-scatter.4.cloned.1.call-update) | async-done | bytes 65552 | tf_op jit(solution)/shard_map/reduce_scatter | solution.py:78
  102.1 1.2 fusion.8
  104.2 0.9 fusion.37
  105.0 5.4 %all_gather.10 = bf16[128,512]{1,0:T(8,128)(2,1)S(1)} all-gather(bf16[32,512]{1,0:T(8,128)(2,1)S(1)} %fusion.37), channel_id=1, replica_groups=mesh['tp'=8,'dp'=4] {'dp'}, dimensions={0}, use_global_device_ids=true | all-gather | bytes 163840 | tf_op jit(solution)/shard_map/all_gather | solution.py:110
  110.8 43.3 %all-reduce.1 = bf16[128,1024]{1,0:T(8,128)(2,1)S(1)} all-reduce(f32[128,1024]{1,0:T(8,128)S(1)} %fusion.48), channel_id=1, replica_groups=mesh['tp'=8,'dp'=4] {'tp'}, use_global_device_ids=true, to_apply=%region_4.5 | all-reduce | flops 131072 | bytes 786432 | tf_op jit(solution)/shard_map/psum | solution.py:150
  154.2 5.9 %psum.23 = f32[128,1]{0,1:T(1,128)S(1)} all-reduce(f32[128,1]{0,1:T(1,128)S(1)} %bitcast.134), channel_id=1, replica_groups=mesh['tp'=8,'dp'=4] {'dp'}, use_global_device_ids=true, to_apply=%region_6.7 | all-reduce | flops 128 | bytes 1024 | tf_op jit(solution)/shard_map/psum | solution.py:152
  160.2 1.6 convolution_convert_fusion
  161.8 1.6 convolution_convert_fusion.1
  164.5 16.2 %reduce-scatter.6.cloned.1.call-done = bf16[32,1024]{1,0:T(8,128)(2,1)} async-done(((bf16[128,1024]{1,0:T(8,128)(2,1)}), bf16[32,1024]{1,0:T(8,128)(2,1)}) %reduce-scatter.6.cloned.1.call-update) | async-done | bytes 65552 | tf_op jit(solution)/shard_map/reduce_scatter | solution.py:78
  182.5 0.9 fusion.42
  183.4 5.5 %all_gather.11 = bf16[128,512]{1,0:T(8,128)(2,1)S(1)} all-gather(bf16[32,512]{1,0:T(8,128)(2,1)S(1)} %fusion.42), channel_id=1, replica_groups=mesh['tp'=8,'dp'=4] {'dp'}, dimensions={0}, use_global_device_ids=true | all-gather | bytes 163840 | tf_op jit(solution)/shard_map/all_gather | solution.py:110
  190.2 0.9 copy.34
  191.1 0.9 copy.30
  192.1 0.9 copy.42
  194.7 58.8 %reduce-scatter.8.cloned.1.call-done = f32[128,128]{1,0:T(8,128)} async-done(((f32[128,1024]{1,0:T(8,128)}), f32[128,128]{1,0:T(8,128)}) %reduce-scatter.8.cloned.1.call-update) | async-done | bytes 65552 | tf_op jit(solution)/shard_map/reduce_scatter | solution.py:170
  253.5 1.5 convert_element_type.132
  (90 shorter events, 11.3 us)
Async XLA Ops:
  7.2 94.1 %reduce-scatter.4.cloned.1.call-start = ((), (), s32[]{:S(2)}) async-start(), calls=%async_computation.3 | async-start | bytes 327680 | tf_op jit(solution)/shard_map/reduce_scatter | solution.py:78
  78.7 4.0 %copy-start.19 = (f32[2,512]{1,0:T(2,128)S(1)}, f32[2,512]{1,0:T(2,128)}, u32[]{:S(2)}) copy-start(f32[2,512]{1,0:T(2,128)} %param.22) | copy-start | bytes 12292
  78.7 4.0 %copy-start.4 = (bf16[2,256,512]{2,1,0:T(8,128)(2,1)S(1)}, bf16[2,256,512]{2,1,0:T(8,128)(2,1)}, u32[]{:S(2)}) copy-start(bf16[2,256,512]{2,1,0:T(8,128)(2,1)} %param.20) | copy-start | bytes 1572868
  80.3 3.7 %copy-start.20 = (s32[32]{0:T(128)S(1)}, s32[32]{0:T(128)}, u32[]{:S(2)}) copy-start(s32[32]{0:T(128)} %param.13) | copy-start | bytes 388
  82.6 3.0 %copy-start.16 = (bf16[2,4,512]{2,1,0:T(4,128)(2,1)S(1)}, bf16[2,4,512]{2,1,0:T(4,128)(2,1)}, u32[]{:S(2)}) copy-start(bf16[2,4,512]{2,1,0:T(4,128)(2,1)} %param.19) | copy-start | bytes 24580
  82.7 98.0 %reduce-scatter.6.cloned.1.call-start = ((), (), s32[]{:S(2)}) async-start(), calls=%async_computation.4 | async-start | bytes 327680 | tf_op jit(solution)/shard_map/reduce_scatter | solution.py:78
  82.8 21.3 %copy-start.5 = (f32[2,32,512]{2,1,0:T(8,128)S(1)}, f32[2,32,512]{2,1,0:T(8,128)}, u32[]{:S(2)}) copy-start(f32[2,32,512]{2,1,0:T(8,128)} %param.14) | copy-start | bytes 393220
  82.8 27.6 %copy-start.1 = (bf16[2,512,1024]{2,1,0:T(8,128)(2,1)S(1)}, bf16[2,512,1024]{2,1,0:T(8,128)(2,1)}, u32[]{:S(2)}) copy-start(bf16[2,512,1024]{2,1,0:T(8,128)(2,1)} %param.23) | copy-start | bytes 6291460
  85.7 25.1 %copy-start.8 = (bf16[128,128]{1,0:T(8,128)(2,1)S(1)}, bf16[128,128]{1,0:T(8,128)(2,1)}, u32[]{:S(2)}) copy-start(bf16[128,128]{1,0:T(8,128)(2,1)} %param.12) | copy-start | bytes 98308
  86.8 24.0 %copy-start.2 = (bf16[32,3,512]{2,0,1:T(8,128)(2,1)}, bf16[32,3,512]{2,0,1:T(8,128)(2,1)S(1)}, u32[]{:S(2)}) copy-start(bf16[32,3,512]{2,0,1:T(8,128)(2,1)S(1)} %get-tuple-element.8) | copy-start | bytes 294916
  102.1 2.1 copy-start.9
  103.3 0.6 copy-start.12
  104.1 0.9 copy-start.11
  163.4 19.2 %copy-start.6 = (f32[2,32,512]{2,1,0:T(8,128)S(1)}, f32[2,32,512]{2,1,0:T(8,128)}, u32[]{:S(2)}) copy-start(f32[2,32,512]{2,1,0:T(8,128)} %param.14) | copy-start | bytes 393220
  163.4 19.1 %copy-start.17 = (pred[32]{0:T(512)(128)(4,1)S(1)}, pred[32]{0:T(512)(128)(4,1)}, u32[]{:S(2)}) copy-start(pred[32]{0:T(512)(128)(4,1)} %broadcast_compare_fusion.1) | copy-start | bytes 100
  164.1 89.4 %reduce-scatter.8.cloned.1.call-start = ((), (), s32[]{:S(2)}) async-start(), calls=%async_computation.5 | async-start | bytes 589824 | tf_op jit(solution)/shard_map/reduce_scatter | solution.py:170
  181.7 1.7 copy-start.15
  181.7 10.4 %copy-start.3 = (bf16[32,3,512]{2,0,1:T(8,128)(2,1)S(1)}, bf16[32,3,512]{2,0,1:T(8,128)(2,1)}, u32[]{:S(2)}) copy-start(bf16[32,3,512]{2,0,1:T(8,128)(2,1)} %copy-done.2) | copy-start | bytes 294916
  181.9 0.6 copy-start.13
  183.4 9.7 %copy-start.14 = (f32[2,32,256]{2,1,0:T(8,128)S(1)}, f32[2,32,256]{2,1,0:T(8,128)}, u32[]{:S(2)}) copy-start(f32[2,32,256]{2,1,0:T(8,128)} %copy-done.13) | copy-start | bytes 196612
  183.4 9.8 %copy-start.7 = (f32[2,32,512]{2,1,0:T(8,128)S(1)}, f32[2,32,512]{2,1,0:T(8,128)}, u32[]{:S(2)}) copy-start(f32[2,32,512]{2,1,0:T(8,128)} %param.14) | copy-start | bytes 393220
  183.4 9.8 %copy-start.10 = (bf16[32,512]{1,0:T(8,128)(2,1)S(1)}, bf16[32,512]{1,0:T(8,128)(2,1)}, u32[]{:S(2)}) copy-start(bf16[32,512]{1,0:T(8,128)(2,1)} %copy-done.9) | copy-start | bytes 98308
  183.4 9.8 %copy-start.18 = (pred[32]{0:T(512)(128)(4,1)S(1)}, pred[32]{0:T(512)(128)(4,1)}, u32[]{:S(2)}) copy-start(pred[32]{0:T(512)(128)(4,1)} %broadcast_compare_fusion.1) | copy-start | bytes 100
  189.3 0.8 copy-start
Sparse Core Ops, SparseCore 0:
  82.8 18.4 reduce-scatter.3
  164.3 16.3 reduce-scatter.5
  190.3 63.2 reduce-scatter.7
where the time goes:
time: 263 us; the launch traced here: 262 us
  blocking collectives  129 us (49%)
  waiting for transfers between devices  89.6 us (34%)
  between operations  14.3 us (5%)
  local copies, waits for them, and re-layouts  10.4 us (4%)
  other arithmetic  9.79 us (4%)
  matrix products  8.71 us (3%)
    reduce_scatter x1, waiting for transfers between devices, body(): lax.psum_scatter(terms, 'tp', scatter_dimension=1, tiled=True)  58.8 us
    psum x1, blocking collectives, body(): carried = lax.psum(terms, 'tp').astype(jnp.bfloat16)  43.3 us
    psum x1, blocking collectives, normed_input(): lax.psum(jnp.sum(widened * widened, axis=1, keepdims=True), ('tp', 'dp'))  42 us
    reduce_scatter x2, waiting for transfers between devices, recurrent_step(): lax.psum_scatter(jnp.concatenate([jnp.dot(normed, w_branch, preferred_ele...  30.7 us
    all_gather x1, blocking collectives, normed_input(): lax.all_gather(norm_rows(stream_local, own_gain, squares), 'tp', axis=1,...  26.4 us
    all_gather x2, blocking collectives, recurrent_step(): lax.all_gather(readout, 'dp', axis=0, tiled=True)  11 us
    psum x1, blocking collectives, body(): squares = lax.psum(jnp.sum(widened * widened, axis=1, keepdims=True), 'dp')  5.93 us
  transfers between devices with their start and end apart: 3, of which 3 were waited for; matrix products, arithmetic and copies ran while one was open for 3% of the time, Pallas kernels for 0%

commit v1 on v0

--- a/solution.py
+++ b/solution.py
@@ -2,6 +2,7 @@
 import jax.numpy as jnp
 from jax import lax
 from jax.sharding import PartitionSpec as P
+from jax.lax import psum
 
 D = 4096
 BLOCK = 256
@@ -27,7 +28,8 @@
     own_width = stream_local.shape[1]
     offset = lax.axis_index("tp") * own_width
     widened = stream_local.astype(jnp.float32)
-    squares = lax.psum(jnp.sum(widened * widened, axis=1, keepdims=True), ("tp", "dp"))
+    chunk = jnp.sum(widened * widened, axis=1, keepdims=True)
+    squares = psum(psum(chunk, "tp"), "dp")
     own_gain = lax.dynamic_slice_in_dim(gain_block, offset, own_width, 0)
     result = lax.all_gather(norm_rows(stream_local, own_gain, squares), "tp", axis=1, tiled=True)
     return result

time: 263 us -> 249 us (0.947)
  blocking collectives: 129 us -> 115 us
    psum x1 -> x2, blocking collectives: 42 us -> 28.8 us  [normed_input(): squares = psum(psum(chunk, 'tp'), 'dp')]
where the time goes in v1:
time: 249 us; the launch traced here: 247 us
  blocking collectives  115 us (46%)
  waiting for transfers between devices  88.7 us (36%)
  between operations  14.3 us (6%)
  local copies, waits for them, and re-layouts  10.5 us (4%)
  other arithmetic  9.79 us (4%)
  matrix products  8.69 us (3%)
    reduce_scatter x1, waiting for transfers between devices, body(): lax.psum_scatter(terms, 'tp', scatter_dimension=1, tiled=True)  58.8 us
    psum x1, blocking collectives, body(): carried = lax.psum(terms, 'tp').astype(jnp.bfloat16)  43.3 us
    reduce_scatter x2, waiting for transfers between devices, recurrent_step(): lax.psum_scatter(jnp.concatenate([jnp.dot(normed, w_branch, preferred_ele...  29.8 us
    psum x2, blocking collectives, normed_input(): squares = psum(psum(chunk, 'tp'), 'dp')  28.8 us
    all_gather x1, blocking collectives, normed_input(): lax.all_gather(norm_rows(stream_local, own_gain, squares), 'tp', axis=1,...  26.4 us
    all_gather x2, blocking collectives, recurrent_step(): lax.all_gather(readout, 'dp', axis=0, tiled=True)  11 us
    psum x1, blocking collectives, body(): squares = lax.psum(jnp.sum(widened * widened, axis=1, keepdims=True), 'dp')  5.93 us
  transfers between devices with their start and end apart: 3, of which 3 were waited for; matrix products, arithmetic and copies ran while one was open for 3% of the time, Pallas kernels for 0%

profile of v1, /device:TPU:0, one launch (start us, length us, event | category | flops | bytes accessed | tf_op | source)
XLA Modules:
  0.0 247.5 jit_solution(14357538530264192292)
XLA Ops:
  7.2 0.9 fusion.45
  8.1 23.2 %psum.28 = f32[128,1]{0,1:T(1,128)S(1)} all-reduce(f32[128,1]{0,1:T(1,128)S(1)} %bitcast.133), channel_id=1, replica_groups=mesh['tp'=8,'dp'=4] {'tp'}, use_global_device_ids=true, to_apply=%region_1.0 | all-reduce | flops 128 | bytes 1024 | tf_op jit(solution)/shard_map/psum | solution.py:32
  31.2 5.6 %psum.29 = f32[128,1]{0,1:T(1,128)S(1)} all-reduce(f32[128,1]{0,1:T(1,128)S(1)} %psum.28), channel_id=1, replica_groups=mesh['tp'=8,'dp'=4] {'dp'}, use_global_device_ids=true, to_apply=%region_2.0 | all-reduce | flops 128 | bytes 1024 | tf_op jit(solution)/shard_map/psum | solution.py:32
  36.9 1.4 fusion.76
  39.1 26.4 %all_gather.9 = bf16[128,1024]{1,0:T(8,128)(2,1)S(1)} all-gather(bf16[128,128]{1,0:T(8,128)(2,1)S(1)} %fusion.47), channel_id=1, replica_groups=mesh['tp'=8,'dp'=4] {'tp'}, dimensions={1}, use_global_device_ids=true | all-gather | bytes 294912 | tf_op jit(solution)/shard_map/all_gather | solution.py:34
  65.6 1.6 convolution_convert_fusion.2
  67.2 1.5 convolution_convert_fusion.3
  69.7 1.2 fusion.74
  72.5 1.0 bitcast_select_fusion.1
  73.6 13.6 %reduce-scatter.4.cloned.1.call-done = bf16[32,1024]{1,0:T(8,128)(2,1)} async-done(((bf16[128,1024]{1,0:T(8,128)(2,1)}), bf16[32,1024]{1,0:T(8,128)(2,1)}) %reduce-scatter.4.cloned.1.call-update) | async-done | bytes 65552 | tf_op jit(solution)/shard_map/reduce_scatter | solution.py:80
  88.0 1.2 fusion.8
  90.0 0.9 fusion.37
  90.9 5.4 %all_gather.10 = bf16[128,512]{1,0:T(8,128)(2,1)S(1)} all-gather(bf16[32,512]{1,0:T(8,128)(2,1)S(1)} %fusion.37), channel_id=1, replica_groups=mesh['tp'=8,'dp'=4] {'dp'}, dimensions={0}, use_global_device_ids=true | all-gather | bytes 163840 | tf_op jit(solution)/shard_map/all_gather | solution.py:112
  96.7 43.3 %all-reduce.1 = bf16[128,1024]{1,0:T(8,128)(2,1)S(1)} all-reduce(f32[128,1024]{1,0:T(8,128)S(1)} %fusion.48), channel_id=1, replica_groups=mesh['tp'=8,'dp'=4] {'tp'}, use_global_device_ids=true, to_apply=%region_5.6 | all-reduce | flops 131072 | bytes 786432 | tf_op jit(solution)/shard_map/psum | solution.py:152
  140.1 5.9 %psum.31 = f32[128,1]{0,1:T(1,128)S(1)} all-reduce(f32[128,1]{0,1:T(1,128)S(1)} %bitcast.134), channel_id=1, replica_groups=mesh['tp'=8,'dp'=4] {'dp'}, use_global_device_ids=true, to_apply=%region_7.8 | all-reduce | flops 128 | bytes 1024 | tf_op jit(solution)/shard_map/psum | solution.py:154
  146.1 1.6 convolution_convert_fusion
  147.7 1.6 convolution_convert_fusion.1
  150.4 16.2 %reduce-scatter.6.cloned.1.call-done = bf16[32,1024]{1,0:T(8,128)(2,1)} async-done(((bf16[128,1024]{1,0:T(8,128)(2,1)}), bf16[32,1024]{1,0:T(8,128)(2,1)}) %reduce-scatter.6.cloned.1.call-update) | async-done | bytes 65552 | tf_op jit(solution)/shard_map/reduce_scatter | solution.py:80
  169.3 5.5 %all_gather.11 = bf16[128,512]{1,0:T(8,128)(2,1)S(1)} all-gather(bf16[32,512]{1,0:T(8,128)(2,1)S(1)} %fusion.42), channel_id=1, replica_groups=mesh['tp'=8,'dp'=4] {'dp'}, dimensions={0}, use_global_device_ids=true | all-gather | bytes 163840 | tf_op jit(solution)/shard_map/all_gather | solution.py:112
  176.1 0.9 copy.34
  177.0 0.9 copy.30
  178.0 0.9 copy.42
  180.6 58.8 %reduce-scatter.8.cloned.1.call-done = f32[128,128]{1,0:T(8,128)} async-done(((f32[128,1024]{1,0:T(8,128)}), f32[128,128]{1,0:T(8,128)}) %reduce-scatter.8.cloned.1.call-update) | async-done | bytes 65552 | tf_op jit(solution)/shard_map/reduce_scatter | solution.py:172
  239.5 1.5 convert_element_type.132
  (91 shorter events, 12.1 us)
Async XLA Ops:
  7.2 80.0 %reduce-scatter.4.cloned.1.call-start = ((), (), s32[]{:S(2)}) async-start(), calls=%async_computation.3 | async-start | bytes 327680 | tf_op jit(solution)/shard_map/reduce_scatter | solution.py:80
  65.6 4.0 %copy-start.19 = (f32[2,512]{1,0:T(2,128)S(1)}, f32[2,512]{1,0:T(2,128)}, u32[]{:S(2)}) copy-start(f32[2,512]{1,0:T(2,128)} %param.22) | copy-start | bytes 12292
  65.6 4.0 %copy-start.4 = (bf16[2,256,512]{2,1,0:T(8,128)(2,1)S(1)}, bf16[2,256,512]{2,1,0:T(8,128)(2,1)}, u32[]{:S(2)}) copy-start(bf16[2,256,512]{2,1,0:T(8,128)(2,1)} %param.20) | copy-start | bytes 1572868
  67.2 3.7 %copy-start.20 = (s32[32]{0:T(128)S(1)}, s32[32]{0:T(128)}, u32[]{:S(2)}) copy-start(s32[32]{0:T(128)} %param.13) | copy-start | bytes 388
  69.4 3.1 %copy-start.16 = (bf16[2,4,512]{2,1,0:T(4,128)(2,1)S(1)}, bf16[2,4,512]{2,1,0:T(4,128)(2,1)}, u32[]{:S(2)}) copy-start(bf16[2,4,512]{2,1,0:T(4,128)(2,1)} %param.19) | copy-start | bytes 24580
  69.5 97.1 %reduce-scatter.6.cloned.1.call-start = ((), (), s32[]{:S(2)}) async-start(), calls=%async_computation.4 | async-start | bytes 327680 | tf_op jit(solution)/shard_map/reduce_scatter | solution.py:80
  69.6 20.4 %copy-start.5 = (f32[2,32,512]{2,1,0:T(8,128)S(1)}, f32[2,32,512]{2,1,0:T(8,128)}, u32[]{:S(2)}) copy-start(f32[2,32,512]{2,1,0:T(8,128)} %param.14) | copy-start | bytes 393220
  69.6 26.7 %copy-start.1 = (bf16[2,512,1024]{2,1,0:T(8,128)(2,1)S(1)}, bf16[2,512,1024]{2,1,0:T(8,128)(2,1)}, u32[]{:S(2)}) copy-start(bf16[2,512,1024]{2,1,0:T(8,128)(2,1)} %param.23) | copy-start | bytes 6291460
  72.5 24.1 %copy-start.8 = (bf16[128,128]{1,0:T(8,128)(2,1)S(1)}, bf16[128,128]{1,0:T(8,128)(2,1)}, u32[]{:S(2)}) copy-start(bf16[128,128]{1,0:T(8,128)(2,1)} %param.12) | copy-start | bytes 98308
  73.6 23.1 %copy-start.2 = (bf16[32,3,512]{2,0,1:T(8,128)(2,1)}, bf16[32,3,512]{2,0,1:T(8,128)(2,1)S(1)}, u32[]{:S(2)}) copy-start(bf16[32,3,512]{2,0,1:T(8,128)(2,1)S(1)} %get-tuple-element.8) | copy-start | bytes 294916
  88.0 2.1 copy-start.9
  89.2 0.6 copy-start.12
  90.0 0.9 copy-start.11
  149.3 19.2 %copy-start.6 = (f32[2,32,512]{2,1,0:T(8,128)S(1)}, f32[2,32,512]{2,1,0:T(8,128)}, u32[]{:S(2)}) copy-start(f32[2,32,512]{2,1,0:T(8,128)} %param.14) | copy-start | bytes 393220
  149.3 19.2 %copy-start.17 = (pred[32]{0:T(512)(128)(4,1)S(1)}, pred[32]{0:T(512)(128)(4,1)}, u32[]{:S(2)}) copy-start(pred[32]{0:T(512)(128)(4,1)} %broadcast_compare_fusion.1) | copy-start | bytes 100
  150.0 89.4 %reduce-scatter.8.cloned.1.call-start = ((), (), s32[]{:S(2)}) async-start(), calls=%async_computation.5 | async-start | bytes 589824 | tf_op jit(solution)/shard_map/reduce_scatter | solution.py:172
  167.6 1.7 copy-start.15
  167.6 10.4 %copy-start.3 = (bf16[32,3,512]{2,0,1:T(8,128)(2,1)S(1)}, bf16[32,3,512]{2,0,1:T(8,128)(2,1)}, u32[]{:S(2)}) copy-start(bf16[32,3,512]{2,0,1:T(8,128)(2,1)} %copy-done.2) | copy-start | bytes 294916
  167.8 0.6 copy-start.13
  169.3 9.7 %copy-start.14 = (f32[2,32,256]{2,1,0:T(8,128)S(1)}, f32[2,32,256]{2,1,0:T(8,128)}, u32[]{:S(2)}) copy-start(f32[2,32,256]{2,1,0:T(8,128)} %copy-done.13) | copy-start | bytes 196612
  169.3 9.8 %copy-start.7 = (f32[2,32,512]{2,1,0:T(8,128)S(1)}, f32[2,32,512]{2,1,0:T(8,128)}, u32[]{:S(2)}) copy-start(f32[2,32,512]{2,1,0:T(8,128)} %param.14) | copy-start | bytes 393220
  169.3 9.8 %copy-start.10 = (bf16[32,512]{1,0:T(8,128)(2,1)S(1)}, bf16[32,512]{1,0:T(8,128)(2,1)}, u32[]{:S(2)}) copy-start(bf16[32,512]{1,0:T(8,128)(2,1)} %copy-done.9) | copy-start | bytes 98308
  169.3 9.8 %copy-start.18 = (pred[32]{0:T(512)(128)(4,1)S(1)}, pred[32]{0:T(512)(128)(4,1)}, u32[]{:S(2)}) copy-start(pred[32]{0:T(512)(128)(4,1)} %broadcast_compare_fusion.1) | copy-start | bytes 100
  175.2 0.8 copy-start
Sparse Core Ops, SparseCore 0:
  69.6 17.5 reduce-scatter.3
  150.2 16.3 reduce-scatter.5
  176.2 63.2 reduce-scatter.7
